TPU v7x, 32 devices: a whole 2x2x4 slice. The times are simulated.
32 devices in a mesh: ep: 8 (over z, x), tp: 4 (over y, core).
Axes of the slice: x: 2, y: 2, z: 4, core: 2. Of those that a mesh axis runs over, the one named last changes fastest.
Arguments:
- tokens: bfloat16 [1024, 1024], P('ep', 'tp'), may hold values from -6 to 6
- cotangent: bfloat16 [1024, 1024], P('ep', 'tp'), may hold values from -4 to 4
- routes: int32 [1024, 2], P('ep'), may hold values from 0 to 7, all different within a row; in each aligned block of 128 rows (0 to 127, 128 to 255, ...) at most 40 rows name the same one
- route_weights: bfloat16 [1024, 2], P('ep'), may hold values from 0.099609375 to 0.8984375
- w_gate: bfloat16 [8, 1024, 2816], P('ep', None, 'tp'), may hold values from -0.1875 to 0.1875
- w_up: bfloat16 [8, 1024, 2816], P('ep', None, 'tp'), may hold values from -0.1875 to 0.1875
- w_down: bfloat16 [8, 2816, 1024], P('ep', 'tp'), may hold values from -0.109375 to 0.109375
- dense_weight: bfloat16 [1024, 1024], P('tp', 'ep'), may hold values from -0.25 to 0.25
- mix_gate: float32 [1024], replicated, may hold values from 0.1 to 1.9
Outputs:
- token_grad: bfloat16 [1024, 1024], P('ep', 'tp')
- route_grad: float32 [1024, 2], P('ep')
- gate_grad: bfloat16 [8, 1024, 2816], P('ep', None, 'tp')
- up_grad: bfloat16 [8, 1024, 2816], P('ep', None, 'tp')
- down_grad: bfloat16 [8, 2816, 1024], P('ep', 'tp')
- dense_grad: float32 [1024, 1024], P('tp', 'ep')
- mix_grad: float32 [1024], replicated
Inputs may be any that keep to these rules, and one draw needn't show every extreme that they name: `routes`: each row names 2 different experts. In the rows of one index of ep (aligned blocks of 128 rows) no expert is named by more than 40 rows, a bound that some block reaches.
All inputs are finite; a program needn't handle non-finite values.
Results may differ from a plain program's by a relative error of at most 0.0065.
Values may be sent and summed in bfloat16 or wider, within the bound.
A program may use at most 64 MiB of HBM per device.

v0:
```python
import jax
import jax.numpy as jnp
from jax import lax
from jax.sharding import PartitionSpec as P

FF = 2816


def spread(values, experts, group_size):
    capacity = values.shape[0] // experts
    shaped = values.reshape((experts, 1, capacity) + values.shape[1:])
    copies = jnp.broadcast_to(shaped, (experts, group_size, capacity) + values.shape[1:])
    return copies.reshape((experts * group_size * capacity,) + values.shape[1:])


def local(tokens, cotangent, routes, route_weights, w_gate, w_up, w_down, dense_weight, mix_gate):
    tp_count = lax.axis_size("tp")
    ep_count = lax.axis_size("ep")
    slice_width = w_gate.shape[2]
    group_size = FF // (slice_width * tp_count)
    experts = ep_count // group_size
    token_count, top_count = routes.shape
    capacity = 5 * token_count * top_count // (4 * experts)
    picked = routes.reshape(-1)
    onehot = (picked[:, None] == jnp.arange(experts, dtype=jnp.int32)[None, :]).astype(jnp.int32)
    ranking = jnp.cumsum(onehot, axis=0) - 1
    target = picked * capacity + jnp.sum(onehot * ranking, axis=1)
    matches = (target[:, None] == jnp.arange(experts * capacity, dtype=jnp.int32)[None, :]).astype(
        jnp.int32
    )
    pick_index = jnp.arange(picked.shape[0], dtype=jnp.int32)
    pick_of = jnp.sum(matches * pick_index[:, None], axis=0)
    filled = jnp.sum(matches, axis=0)
    token_of = pick_of // top_count
    slot_weight = jnp.take(route_weights.reshape(-1), pick_of, axis=0) * filled.astype(jnp.bfloat16)
    weight_out = spread(slot_weight, experts, group_size)
    grads_full = lax.all_gather(cotangent, "tp", axis=1, tiled=True)
    rows_part, grads_in, weights_in = (
        lax.all_to_all(
            spread(jnp.take(tokens, token_of, axis=0), experts, group_size),
            "ep",
            split_axis=0,
            concat_axis=0,
            tiled=True,
        ),
        lax.all_to_all(
            spread(jnp.take(grads_full, token_of, axis=0), experts, group_size),
            "ep",
            split_axis=0,
            concat_axis=0,
            tiled=True,
        ),
        lax.all_to_all(weight_out, "ep", split_axis=0, concat_axis=0, tiled=True),
    )
    rows_in = lax.all_gather(rows_part, "tp", axis=1, tiled=True)
    gate_matrix = w_gate[0]
    up_matrix = w_up[0]
    down_matrix = w_down[0]
    pre_gate = jnp.dot(rows_in, gate_matrix, preferred_element_type=jnp.float32)
    pre_up = jnp.dot(rows_in, up_matrix, preferred_element_type=jnp.float32)
    sigmoid_gate = jax.nn.sigmoid(pre_gate)
    activated = pre_gate * sigmoid_gate
    hidden = activated * pre_up
    hidden_bf = hidden.astype(jnp.bfloat16)
    projected = lax.dot_general(
        grads_in, down_matrix, (((1,), (1,)), ((), ())), preferred_element_type=jnp.float32
    )
    route_part = jnp.sum(hidden_bf.astype(jnp.float32) * projected, axis=1)
    weight_col = weights_in.astype(jnp.float32)[:, None]
    hidden_grad = weight_col * projected
    d_gate = (hidden_grad * pre_up * sigmoid_gate * (1.0 + pre_gate * (1.0 - sigmoid_gate))).astype(
        jnp.bfloat16
    )
    d_up = (hidden_grad * activated).astype(jnp.bfloat16)
    weighted = (weight_col * hidden).astype(jnp.bfloat16)
    contract_rows = (((0,), (0,)), ((), ()))
    gate_grad = lax.dot_general(
        rows_in, d_gate, contract_rows, preferred_element_type=jnp.float32
    ).astype(jnp.bfloat16)[None]
    up_grad = lax.dot_general(
        rows_in, d_up, contract_rows, preferred_element_type=jnp.float32
    ).astype(jnp.bfloat16)[None]
    down_grad = lax.dot_general(
        weighted, grads_in, contract_rows, preferred_element_type=jnp.float32
    ).astype(jnp.bfloat16)[None]
    contract_cols = (((1,), (1,)), ((), ()))
    partial_value = (
        lax.dot_general(d_gate, gate_matrix, contract_cols, preferred_element_type=jnp.float32)
        + lax.dot_general(d_up, up_matrix, contract_cols, preferred_element_type=jnp.float32)
    ).astype(jnp.bfloat16)
    mixed = lax.all_to_all(partial_value, "tp", split_axis=1, concat_axis=0, tiled=True)
    rows_here = partial_value.shape[0]
    column_sum = jnp.sum(mixed.reshape(tp_count, rows_here, -1).astype(jnp.float32), axis=0).astype(
        jnp.bfloat16
    )
    route_sum = lax.psum(route_part, "tp")
    returned = lax.all_to_all(column_sum, "ep", split_axis=0, concat_axis=0, tiled=True)
    route_back = lax.all_to_all(route_sum, "ep", split_axis=0, concat_axis=0, tiled=True)
    slot_grad = jnp.sum(
        returned.reshape(experts, group_size, capacity, -1).astype(jnp.float32), axis=1
    ).reshape(experts * capacity, -1)
    slot_route = jnp.sum(route_back.reshape(experts, group_size, capacity), axis=1).reshape(-1)
    expert_grad = jnp.sum(
        jnp.take(slot_grad, target, axis=0).reshape(token_count, top_count, -1), axis=1
    )
    route_grad = jnp.take(slot_route, target, axis=0).reshape(token_count, top_count)
    scaled = (mix_gate[None, :] * grads_full.astype(jnp.float32)).astype(jnp.bfloat16)
    moment = lax.dot_general(tokens, grads_full, contract_rows, preferred_element_type=jnp.float32)
    shard_piece = lax.all_gather(dense_weight, "ep", axis=1, tiled=True)
    scaled_cols = scaled
    dense_acc = lax.dot_general(
        scaled_cols, shard_piece, contract_cols, preferred_element_type=jnp.float32
    )
    gain_cols = jnp.sum(shard_piece.astype(jnp.float32) * moment, axis=0)
    gain_part = gain_cols
    dense_dx, gain_part = (dense_acc, gain_part)
    mix_grad = lax.psum(gain_part, ("ep", "tp")) / ep_count
    scaled_cols = scaled
    product = lax.dot_general(
        scaled_cols, tokens, contract_rows, preferred_element_type=jnp.float32
    )
    dense_rows_sum = lax.psum_scatter(
        product * (1.0 / ep_count), "ep", scatter_dimension=0, tiled=True
    )
    dense_grad = dense_rows_sum.T
    token_grad = (expert_grad + dense_dx).astype(jnp.bfloat16)
    return (token_grad, route_grad, gate_grad, up_grad, down_grad, dense_grad, mix_grad)


def solution(mesh):
    return jax.shard_map(
        local,
        mesh=mesh,
        in_specs=(
            P("ep", "tp"),
            P("ep", "tp"),
            P("ep", None),
            P("ep", None),
            P("ep", None, "tp"),
            P("ep", None, "tp"),
            P("ep", "tp", None),
            P("tp", "ep"),
            P(),
        ),
        out_specs=(
            P("ep", "tp"),
            P("ep", None),
            P("ep", None, "tp"),
            P("ep", None, "tp"),
            P("ep", "tp", None),
            P("tp", "ep"),
            P(),
        ),
        check_vma=False,
    )
```

profile of v0, /device:TPU:0, one launch (start us, length us, event | category | flops | bytes accessed | tf_op | source)
XLA Modules:
  0.0 188.5 jit_solution(2119766287538482815)
XLA Ops:
  7.2 0.9 copy.33
  8.4 0.6 reduce-window.6
  9.0 0.2 slice_reduce_fusion
  9.4 0.2 convert_reduce_fusion
  9.7 0.8 copy.36
  10.7 2.4 %gather_fusion = bf16[320]{0:T(512)(128)(2,1)S(1)} fusion(bf16[256]{0:T(256)(128)(2,1)S(1)} %reshape.281, s32[1024]{0:T(1024)S(1)} %pad_clamp_fusion.2), kind=kCustom, calls=%fused_computation | custom fusion | bytes 2560 | tf_op jit(solution)/shard_map/jit(_take)/gather | solution.py:35
  13.2 0.6 copy.37
  13.8 7.3 %all-to-all-start = ((bf16[8,40,1]{1,2,0:T(2,128)(2,1)}), bf16[8,40,1]{1,2,0:T(2,128)(2,1)S(1)}, u32[]{:S(2)}, u32[]{:S(2)}) async-start(bf16[8,40,1]{1,2,0:T(2,128)(2,1)} %copy.37), calls=%async_computation | async-start | bytes 8192 | tf_op jit(solution)/shard_map/all_to_all | solution.py:53
  21.1 5.8 %all_gather.9 = bf16[128,1024]{1,0:T(8,128)(2,1)S(1)} all-gather(bf16[128,256]{1,0:T(8,128)(2,1)S(1)} %copy-done.6), channel_id=1, replica_groups=mesh['ep'=8,'tp'=4] {'tp'}, dimensions={1}, use_global_device_ids=true | all-gather | bytes 327680 | tf_op jit(solution)/shard_map/all_gather | solution.py:37
  26.9 1.3 convolution_multiply_fusion.1
  28.4 2.0 %gather_fusion.2 = bf16[320,256]{1,0:T(8,128)(2,1)S(1)} fusion(bf16[128,256]{1,0:T(8,128)(2,1)S(1)} %copy-done.1, s32[1024]{0:T(1024)S(1)} %pad_clamp_fusion.1), kind=kCustom, calls=%fused_computation.2 | custom fusion | bytes 328960 | tf_op jit(solution)/shard_map/jit(_take)/gather | solution.py:40
  30.4 29.6 %all_gather.11 = bf16[256,1024]{1,0:T(8,128)(2,1)S(1)} all-gather(bf16[256,128]{1,0:T(8,128)(2,1)S(1)} %copy-done.7), channel_id=1, replica_groups=mesh['ep'=8,'tp'=4] {'ep'}, dimensions={1}, use_global_device_ids=true | all-gather | bytes 589824 | tf_op jit(solution)/shard_map/all_gather | solution.py:109
  60.0 0.8 broadcast_select_fusion.1
  60.8 3.8 %all-to-all-start.2 = ((bf16[8,40,256]{2,1,0:T(8,128)(2,1)}), bf16[8,40,256]{2,1,0:T(8,128)(2,1)S(1)}, u32[]{:S(2)}, u32[]{:S(2)}) async-start(bf16[8,40,256]{2,1,0:T(8,128)(2,1)} %broadcast_select_fusion.1), calls=%async_computation.2 | async-start | bytes 327680 | tf_op jit(solution)/shard_map/all_to_all | solution.py:39
  64.7 0.3 fusion.19
  65.0 2.1 %gather_fusion.1 = bf16[320,1024]{1,0:T(8,128)(2,1)S(1)} fusion(bf16[128,1024]{1,0:T(8,128)(2,1)S(1)} %all_gather.9, s32[1024]{0:T(1024)S(1)} %pad_clamp_fusion.1), kind=kCustom, calls=%fused_computation.1 | custom fusion | bytes 1312000 | tf_op jit(solution)/shard_map/jit(_take)/gather | solution.py:47
  67.2 41.1 %psum.15 = f32[1024]{0:T(1024)S(1)} all-reduce(f32[1024]{0:T(1024)S(1)} %fusion.19), channel_id=1, replica_groups=mesh['ep'=8,'tp'=4] {'ep','tp'}, use_global_device_ids=true, to_apply=%region_11.12 | all-reduce | flops 1024 | bytes 8192 | tf_op jit(solution)/shard_map/psum | solution.py:117
  108.3 1.0 broadcast_select_fusion
  109.3 5.3 %all-to-all-start.1 = ((bf16[8,40,1024]{2,1,0:T(8,128)(2,1)}), bf16[8,40,1024]{2,1,0:T(8,128)(2,1)S(1)}, u32[]{:S(2)}, u32[]{:S(2)}) async-start(bf16[8,40,1024]{2,1,0:T(8,128)(2,1)} %broadcast_select_fusion), calls=%async_computation.1 | async-start | bytes 1310720 | tf_op jit(solution)/shard_map/all_to_all | solution.py:46
  114.6 0.6 broadcast_multiply_fusion.1
  115.3 7.0 %all_gather.10 = bf16[320,1024]{1,0:T(8,128)(2,1)S(1)} all-gather(bf16[320,256]{1,0:T(8,128)(2,1)S(1)} %bitcast.66), channel_id=1, replica_groups=mesh['ep'=8,'tp'=4] {'tp'}, dimensions={1}, use_global_device_ids=true | all-gather | bytes 819200 | tf_op jit(solution)/shard_map/all_gather | solution.py:55
  122.3 1.7 fusion.5
  124.0 1.7 fusion.9
  125.6 4.6 %all-to-all-done.1 = bf16[8,40,1024]{2,1,0:T(8,128)(2,1)S(1)} async-done(((bf16[8,40,1024]{2,1,0:T(8,128)(2,1)}), bf16[8,40,1024]{2,1,0:T(8,128)(2,1)S(1)}, u32[]{:S(2)}, u32[]{:S(2)}) %all-to-all-start.1) | async-done | bytes 655392 | tf_op jit(solution)/shard_map/all_to_all | solution.py:46
  130.2 3.3 %multiply_reduce_fusion = (f32[320]{0:T(512)S(1)}, bf16[320,704]{1,0:T(8,128)(2,1)S(1)}, bf16[320,704]{1,0:T(8,128)(2,1)S(1)}) fusion(f32[320,704]{1,0:T(8,128)} %fusion.9, f32[320,704]{1,0:T(8,128)} %fusion.5, f32[320]{0:T(512)S(1)} %reshape.283, bf16[320,1024]{1,0:T(8,128)(2,1)S(1)} %bitcast.64, bf16[1,704,1024]{2,1,0:T(8,128)(2,1)} %param.15), kind=kOutput, calls=%fused_computation.29 | convolution fusion | flops 465653440 | bytes 4803072 | tf_op jit(solution)/shard_map/dot_general | solution.py:65
  133.6 0.7 fusion.3
  134.3 0.8 copy-done.3
  135.1 0.7 fusion.16
  135.8 0.9 copy.44
  136.7 3.5 %all-to-all-start.3 = ((bf16[320,4,256]{2,0,1:T(8,128)(2,1)}), bf16[320,4,256]{2,0,1:T(8,128)(2,1)S(1)}, u32[]{:S(2)}, u32[]{:S(2)}) async-start(bf16[320,4,256]{2,0,1:T(8,128)(2,1)} %bitcast.61), calls=%async_computation.3 | async-start | bytes 1310720 | tf_op jit(solution)/shard_map/all_to_all | solution.py:91
  140.4 12.0 %psum.14 = f32[8,40,1]{1,0,2:T(8,128)} all-reduce(f32[8,40,1]{1,0,2:T(8,128)S(1)} %all_to_all.47), channel_id=1, replica_groups=mesh['ep'=8,'tp'=4] {'tp'}, use_global_device_ids=true, to_apply=%region_8.9 | all-reduce | flops 320 | bytes 2560 | tf_op jit(solution)/shard_map/psum | solution.py:96
  152.4 3.8 %fusion.2 = bf16[1,704,1024]{2,1,0:T(8,128)(2,1)} fusion(bf16[320,1024]{1,0:T(8,128)(2,1)} %bitcast.65, f32[320]{0:T(512)S(1)} %reshape.283, f32[320,704]{1,0:T(8,128)} %fusion.9, f32[320,704]{1,0:T(8,128)} %fusion.5), kind=kOutput, calls=%fused_computation.10 | convolution fusion | flops 463671296 | bytes 3900672 | tf_op jit(solution)/shard_map/dot_general | solution.py:83
  156.2 3.7 %all-to-all-start.5 = ((f32[8,40,1]{1,2,0:T(1,128)}), f32[8,40,1]{1,2,0:T(1,128)S(1)}, u32[]{:S(2)}, u32[]{:S(2)}) async-start(f32[8,40,1]{1,2,0:T(1,128)} %bitcast.13), calls=%async_computation.5 | async-start | bytes 8192 | tf_op jit(solution)/shard_map/all_to_all | solution.py:98
  159.9 3.1 %fusion.1 = bf16[1,1024,704]{1,2,0:T(8,128)(2,1)} fusion(bf16[320,1024]{1,0:T(8,128)(2,1)} %copy-done.4, bf16[320,704]{1,0:T(8,128)(2,1)S(1)} %get-tuple-element.43), kind=kOutput, calls=%fused_computation.9 | convolution fusion | flops 462094336 | bytes 2547712 | tf_op jit(solution)/shard_map/dot_general | solution.py:80
  163.1 0.8 reduce_sum.91
  163.9 2.5 %all-to-all-done.5 = f32[8,40,1]{1,2,0:T(1,128)S(1)} async-done(((f32[8,40,1]{1,2,0:T(1,128)}), f32[8,40,1]{1,2,0:T(1,128)S(1)}, u32[]{:S(2)}, u32[]{:S(2)}) %all-to-all-start.5) | async-done | bytes 1312 | tf_op jit(solution)/shard_map/all_to_all | solution.py:98
  166.3 3.6 %all-to-all-start.4 = ((bf16[8,40,256]{2,1,0:T(8,128)(2,1)}), bf16[8,40,256]{2,1,0:T(8,128)(2,1)S(1)}, u32[]{:S(2)}, u32[]{:S(2)}) async-start(bf16[8,40,256]{2,1,0:T(8,128)(2,1)} %bitcast.9), calls=%async_computation.4 | async-start | bytes 327680 | tf_op jit(solution)/shard_map/all_to_all | solution.py:97
  169.9 3.3 %fusion = bf16[1,1024,704]{1,2,0:T(8,128)(2,1)} fusion(bf16[320,1024]{1,0:T(8,128)(2,1)} %copy-done.4, bf16[320,704]{1,0:T(8,128)(2,1)} %copy-done.9), kind=kOutput, calls=%fused_computation.8 | convolution fusion | flops 462094336 | bytes 2547712 | tf_op jit(solution)/shard_map/dot_general | solution.py:77
  173.2 0.5 broadcast.294
  173.7 0.7 reduce.16
  174.5 1.9 %gather_fusion.4 = f32[256]{0:T(256)S(1)} fusion(f32[320]{0:T(512)S(1)} %reshape.282, s32[1024]{0:T(1024)S(1)} %pad_clamp_fusion), kind=kCustom, calls=%fused_computation.4 | custom fusion | bytes 3072 | tf_op jit(solution)/shard_map/jit(_take)/gather | solution.py:106
  176.6 0.6 copy.40
  177.2 0.2 all-to-all-done.4
  177.5 1.0 gather_fusion.3
  178.4 0.1 gather.37
  178.6 0.4 select_reduce_fusion.1
  179.0 0.9 fusion.20
  180.0 1.7 copy.41
  (55 shorter events, 1.9 us)
Async XLA Ops:
  7.2 115.1 %copy-start = (bf16[1,1024,704]{1,2,0:T(8,128)(2,1)S(1)}, bf16[1,1024,704]{1,2,0:T(8,128)(2,1)}, u32[]{:S(2)}) copy-start(bf16[1,1024,704]{1,2,0:T(8,128)(2,1)} %param.13) | copy-start | bytes 4325380
  7.2 13.9 %copy-start.6 = (bf16[128,256]{1,0:T(8,128)(2,1)S(1)}, bf16[128,256]{1,0:T(8,128)(2,1)}, u32[]{:S(2)}) copy-start(bf16[128,256]{1,0:T(8,128)(2,1)} %param.10) | copy-start | bytes 196612
  7.2 19.7 %copy-start.1 = (bf16[128,256]{1,0:T(8,128)(2,1)S(1)}, bf16[128,256]{1,0:T(8,128)(2,1)}, u32[]{:S(2)}) copy-start(bf16[128,256]{1,0:T(8,128)(2,1)} %param.9) | copy-start | bytes 196612
  7.2 19.7 %copy-start.8 = (f32[1024]{0:T(1024)S(1)}, f32[1024]{0:T(1024)}, u32[]{:S(2)}) copy-start(f32[1024]{0:T(1024)} %param.17) | copy-start | bytes 12292
  13.8 47.0 %all-to-all-start = ((bf16[8,40,1]{1,2,0:T(2,128)(2,1)}), bf16[8,40,1]{1,2,0:T(2,128)(2,1)S(1)}, u32[]{:S(2)}, u32[]{:S(2)}) async-start(bf16[8,40,1]{1,2,0:T(2,128)(2,1)} %copy.37), calls=%async_computation | async-start | bytes 8192 | tf_op jit(solution)/shard_map/all_to_all | solution.py:53
  21.1 158.9 %reduce-scatter.2.cloned.1.call-start = ((), (), s32[]{:S(2)}) async-start(), calls=%async_computation.7 | async-start | bytes 1179648 | tf_op jit(solution)/shard_map/reduce_scatter | solution.py:122
  28.2 2.2 %copy-start.7 = (bf16[256,128]{1,0:T(8,128)(2,1)S(1)}, bf16[256,128]{1,0:T(8,128)(2,1)}, u32[]{:S(2)}) copy-start(bf16[256,128]{1,0:T(8,128)(2,1)} %param.16) | copy-start | bytes 196612
  60.8 48.5 %all-to-all-start.2 = ((bf16[8,40,256]{2,1,0:T(8,128)(2,1)}), bf16[8,40,256]{2,1,0:T(8,128)(2,1)S(1)}, u32[]{:S(2)}, u32[]{:S(2)}) async-start(bf16[8,40,256]{2,1,0:T(8,128)(2,1)} %broadcast_select_fusion.1), calls=%async_computation.2 | async-start | bytes 327680 | tf_op jit(solution)/shard_map/all_to_all | solution.py:39
  109.3 20.9 %all-to-all-start.1 = ((bf16[8,40,1024]{2,1,0:T(8,128)(2,1)}), bf16[8,40,1024]{2,1,0:T(8,128)(2,1)S(1)}, u32[]{:S(2)}, u32[]{:S(2)}) async-start(bf16[8,40,1024]{2,1,0:T(8,128)(2,1)} %broadcast_select_fusion), calls=%async_computation.1 | async-start | bytes 1310720 | tf_op jit(solution)/shard_map/all_to_all | solution.py:46
  122.3 1.7 copy-start.4
  122.3 1.7 copy-start.2
  130.2 3.3 %copy-start.5 = (bf16[8,40,1024]{2,1,0:T(8,128)(2,1)}, bf16[8,40,1024]{2,1,0:T(8,128)(2,1)S(1)}, u32[]{:S(2)}) copy-start(bf16[8,40,1024]{2,1,0:T(8,128)(2,1)S(1)} %all-to-all-done.1) | copy-start | bytes 1966084
  133.6 0.8 copy-start.9
  133.6 1.5 copy-start.3
  136.7 19.6 %all-to-all-start.3 = ((bf16[320,4,256]{2,0,1:T(8,128)(2,1)}), bf16[320,4,256]{2,0,1:T(8,128)(2,1)S(1)}, u32[]{:S(2)}, u32[]{:S(2)}) async-start(bf16[320,4,256]{2,0,1:T(8,128)(2,1)} %bitcast.61), calls=%async_computation.3 | async-start | bytes 1310720 | tf_op jit(solution)/shard_map/all_to_all | solution.py:91
  156.2 10.1 %all-to-all-start.5 = ((f32[8,40,1]{1,2,0:T(1,128)}), f32[8,40,1]{1,2,0:T(1,128)S(1)}, u32[]{:S(2)}, u32[]{:S(2)}) async-start(f32[8,40,1]{1,2,0:T(1,128)} %bitcast.13), calls=%async_computation.5 | async-start | bytes 8192 | tf_op jit(solution)/shard_map/all_to_all | solution.py:98
  166.3 11.1 %all-to-all-start.4 = ((bf16[8,40,256]{2,1,0:T(8,128)(2,1)}), bf16[8,40,256]{2,1,0:T(8,128)(2,1)S(1)}, u32[]{:S(2)}, u32[]{:S(2)}) async-start(bf16[8,40,256]{2,1,0:T(8,128)(2,1)} %bitcast.9), calls=%async_computation.4 | async-start | bytes 327680 | tf_op jit(solution)/shard_map/all_to_all | solution.py:97
Sparse Core Ops, SparseCore 0:
  28.4 67.2 reduce-scatter.1
where the time goes:
time: 189 us; the launch traced here: 188 us
  blocking collectives  95.5 us (51%)
  starting transfers between devices  27.2 us (14%)
  matrix products  20.9 us (11%)
  local copies, waits for them, and re-layouts  18 us (10%)
  between operations  14.3 us (8%)
  waiting for transfers between devices  7.31 us (4%)
  other arithmetic  5.3 us (3%)
    psum x1, blocking collectives, local(): mix_grad = lax.psum(gain_part, ('ep', 'tp')) / ep_count  41.1 us
    all_gather x1, blocking collectives, local(): shard_piece = lax.all_gather(dense_weight, 'ep', axis=1, tiled=True)  29.6 us
    psum x1, blocking collectives, local(): route_sum = lax.psum(route_part, 'tp')  12 us
    all_to_all x1, starting transfers between devices, local(): lax.all_to_all(weight_out, 'ep', split_axis=0, concat_axis=0, tiled=True)  7.28 us
    all_gather x1, blocking collectives, local(): rows_in = lax.all_gather(rows_part, 'tp', axis=1, tiled=True)  6.98 us
    all_gather x1, blocking collectives, local(): grads_full = lax.all_gather(cotangent, 'tp', axis=1, tiled=True)  5.78 us
    all_to_all x1, starting transfers between devices, local(): lax.all_to_all(spread(jnp.take(grads_full, token_of, axis=0), experts, gr...  5.31 us
    unnamed x24, local copies, waits for them, and re-layouts  4.87 us
  transfers between devices with their start and end apart: 7, of which 3 were waited for; matrix products, arithmetic and copies ran while one was open for 19% of the time, Pallas kernels for 0%

commit v1 on v0

v1 whole, which is shorter than its diff:
```python
import jax
import jax.numpy as jnp
from jax import lax
from jax.sharding import PartitionSpec as P

FF = 2816
BF = jnp.bfloat16
F32 = jnp.float32


def spread(values, group_size):
    experts = values.shape[0]
    copies = jnp.broadcast_to(values[:, None], (experts, group_size) + values.shape[1:])
    return copies.reshape((experts * group_size,) + values.shape[1:])


def swap(values, axis):
    return lax.all_to_all(values, axis, split_axis=0, concat_axis=0, tiled=True)


def local(tokens, cotangent, routes, route_weights, w_gate, w_up, w_down, dense_weight, mix_gate):
    tp_count = lax.axis_size("tp")
    ep_count = lax.axis_size("ep")
    slice_width = w_gate.shape[2]
    group_size = FF // (slice_width * tp_count)
    experts = ep_count // group_size
    token_count, top_count = routes.shape
    width_part = tokens.shape[1]
    width = width_part * tp_count
    capacity = 5 * token_count * top_count // (4 * experts)
    slots = experts * capacity
    rows_here = ep_count * capacity

    expert_ids = jnp.arange(experts, dtype=jnp.int32)
    named = routes[:, :, None] == expert_ids[None, None, :]
    member = jnp.any(named, axis=1)
    token_ids = jnp.arange(token_count, dtype=jnp.int32)
    before = (token_ids[:, None] > token_ids[None, :]).astype(BF)
    rank = jnp.dot(before, member.astype(BF), preferred_element_type=F32)
    weight_of = jnp.sum(jnp.where(named, route_weights.astype(F32)[:, :, None], 0.0), axis=1)
    slot_ids = jnp.arange(capacity, dtype=jnp.int32).astype(F32)
    rank_t = jnp.where(member, rank, -1.0).T
    hit = rank_t[:, None, :] == slot_ids[None, :, None]
    dispatch = hit.astype(BF).reshape(slots, token_count)
    slot_weight = jnp.sum(jnp.where(hit, weight_of.T[:, None, :], 0.0), axis=2).astype(BF)

    def pick(values):
        taken = jnp.dot(dispatch, values, preferred_element_type=F32).astype(BF)
        return spread(taken.reshape(experts, capacity, values.shape[1]), group_size)

    weights_in = swap(spread(slot_weight, group_size)[:, None, :], "ep").reshape(rows_here)
    rows_part = swap(pick(tokens), "ep")
    grads_full = lax.all_gather(cotangent, "tp", axis=1, tiled=True)
    grads_in = swap(pick(grads_full), "ep").reshape(rows_here, width)
    rows_in = lax.all_gather(rows_part.reshape(rows_here, width_part), "tp", axis=1, tiled=True)

    dense_late, _ = lax.optimization_barrier((dense_weight, rows_part))
    dense_cols = dense_late.shape[1]
    gathered = swap(jnp.broadcast_to(dense_late[None], (ep_count,) + dense_late.shape), "ep")
    scaled = (mix_gate[None, :] * grads_full.astype(F32)).astype(BF)
    contract_rows = (((0,), (0,)), ((), ()))
    contract_cols = (((1,), (1,)), ((), ()))
    product = lax.dot_general(tokens, scaled, contract_rows, preferred_element_type=F32).astype(BF)
    product = product.reshape(width_part, ep_count, dense_cols).transpose(1, 0, 2)

    gate_matrix = w_gate[0]
    up_matrix = w_up[0]
    down_matrix = w_down[0]
    pre_gate = jnp.dot(rows_in, gate_matrix, preferred_element_type=F32)
    pre_up = jnp.dot(rows_in, up_matrix, preferred_element_type=F32)
    sigmoid_gate = jax.nn.sigmoid(pre_gate)
    activated = pre_gate * sigmoid_gate
    hidden = activated * pre_up
    hidden_bf = hidden.astype(BF)
    projected = lax.dot_general(grads_in, down_matrix, contract_cols, preferred_element_type=F32)
    route_part = jnp.sum(hidden_bf.astype(F32) * projected, axis=1)
    weight_col = weights_in.astype(F32)[:, None]
    hidden_grad = weight_col * projected
    d_gate = (hidden_grad * pre_up * sigmoid_gate * (1.0 + pre_gate * (1.0 - sigmoid_gate))).astype(BF)
    d_up = (hidden_grad * activated).astype(BF)
    weighted = (weight_col * hidden).astype(BF)
    partial_value = (
        lax.dot_general(d_gate, gate_matrix, contract_cols, preferred_element_type=F32)
        + lax.dot_general(d_up, up_matrix, contract_cols, preferred_element_type=F32)
    ).astype(BF)
    mixed = lax.all_to_all(partial_value, "tp", split_axis=1, concat_axis=0, tiled=True)
    column_sum = jnp.sum(mixed.reshape(tp_count, rows_here, -1).astype(F32), axis=0).astype(BF)
    returned = swap(column_sum.reshape(ep_count, capacity, width_part), "ep")

    product_late, _ = lax.optimization_barrier((product, grads_in))
    shares = swap(product_late, "ep")
    dense_grad = jnp.sum(shares.astype(F32), axis=0) * (1.0 / ep_count)

    moment = lax.dot_general(tokens, grads_full, contract_rows, preferred_element_type=F32)
    moment = moment.reshape(width_part, ep_count, dense_cols)
    gain = jnp.sum(gathered.astype(F32) * moment.transpose(1, 0, 2), axis=1).reshape(1, width)
    devices = ep_count * tp_count
    route_rows = jnp.broadcast_to(
        route_part.reshape(ep_count, 1, capacity), (ep_count, tp_count, capacity)
    ).reshape(devices, capacity)
    packed = jnp.concatenate([jnp.broadcast_to(gain, (devices, width)), route_rows], axis=1)
    small = swap(packed[:, None, :], ("ep", "tp")).reshape(devices, width + capacity)
    mix_grad = jnp.sum(small[:, :width], axis=0) * (1.0 / ep_count)
    slot_route = jnp.sum(
        small[:, width:].reshape(experts, group_size * tp_count, capacity), axis=1
    )
    expert_route = jnp.sum(jnp.where(hit, slot_route[:, :, None], 0.0), axis=1).T
    route_grad = jnp.sum(jnp.where(named, expert_route[:, None, :], 0.0), axis=2)

    gate_grad = lax.dot_general(rows_in, d_gate, contract_rows, preferred_element_type=F32)
    up_grad = lax.dot_general(rows_in, d_up, contract_rows, preferred_element_type=F32)
    down_grad = lax.dot_general(weighted, grads_in, contract_rows, preferred_element_type=F32)

    back = returned.reshape(experts, group_size, capacity, width_part)
    combine = jnp.broadcast_to(hit[:, None], (experts, group_size) + hit.shape[1:]).astype(BF)
    expert_grad = lax.dot_general(
        combine.reshape(rows_here, token_count),
        back.reshape(rows_here, width_part),
        contract_rows,
        preferred_element_type=F32,
    )
    whole_weight = gathered.transpose(1, 0, 2).reshape(width_part, width)
    dense_dx = lax.dot_general(scaled, whole_weight, contract_cols, preferred_element_type=F32)
    token_grad = (expert_grad + dense_dx).astype(BF)
    return (
        token_grad,
        route_grad,
        gate_grad.astype(BF)[None],
        up_grad.astype(BF)[None],
        down_grad.astype(BF)[None],
        dense_grad,
        mix_grad,
    )


def solution(mesh):
    return jax.shard_map(
        local,
        mesh=mesh,
        in_specs=(
            P("ep", "tp"),
            P("ep", "tp"),
            P("ep", None),
            P("ep", None),
            P("ep", None, "tp"),
            P("ep", None, "tp"),
            P("ep", "tp", None),
            P("tp", "ep"),
            P(),
        ),
        out_specs=(
            P("ep", "tp"),
            P("ep", None),
            P("ep", None, "tp"),
            P("ep", None, "tp"),
            P("ep", "tp", None),
            P("tp", "ep"),
            P(),
        ),
        check_vma=False,
    )
```

time: 189 us -> 135 us (0.71)
  blocking collectives: 95.5 us -> 23.4 us
  waiting for transfers between devices: 7.31 us -> 43.2 us
  between operations: 14.3 us -> 1.06 us
  local copies, waits for them, and re-layouts: 18 us -> 5.96 us
  starting transfers between devices: 27.2 us -> 31.1 us
  other arithmetic: 5.3 us -> 7.9 us
    psum x2 -> x0, blocking collectives: 53.1 us -> none  [the longest x1 41.1 us: local(): mix_grad = lax.psum(gain_part, ('ep', 'tp')) / ep_count]
    all_gather x2 -> x1, blocking collectives: 36.6 us -> 8.36 us  [local(): lax.all_gather(rows_part.reshape(rows_here, width_part), 'tp', axis=1, ti...]
    all_to_all x5 -> x6, waiting for transfers between devices: 7.29 us -> 35 us  [swap(): return lax.all_to_all(values, axis, split_axis=0, concat_axis=0, tiled=True)]
    gather x8 -> x0, local copies, waits for them, and re-layouts: 9.76 us -> none  [the longest x2 2.45 us: local(): jnp.take(route_weights.reshape(-1), pick_of, axis=0)]
    all_to_all x0 -> x1, blocking collectives: none -> 9.1 us  [swap(): return lax.all_to_all(values, axis, split_axis=0, concat_axis=0, tiled=True)]
    all_to_all x1, waiting for transfers between devices: 0.01 us -> 8.21 us  [local(): lax.all_to_all(partial_value, 'tp', split_axis=1, concat_axis=0, tiled=True)]
    all_to_all x5 -> x6, starting transfers between devices: 23.7 us -> 27.6 us  [swap(): return lax.all_to_all(values, axis, split_axis=0, concat_axis=0, tiled=True)]
    reduce_sum x4 -> x8, other arithmetic: 1.49 us -> 3.57 us  [the longest x1 1.27 us: local(): jnp.sum(jnp.where(named, expert_route[:, None, :], 0.0), axis=2)]
  transfers between devices with their start and end apart: 7 -> 7, of which waited for: 3 -> 7; matrix products, arithmetic and copies ran while one was open for 19% -> 16% of each run, Pallas kernels for 0% -> 0%
where the time goes in v1:
time: 135 us; the launch traced here: 134 us
  waiting for transfers between devices  43.2 us (32%)
  starting transfers between devices  31.1 us (23%)
  blocking collectives  23.4 us (17%)
  matrix products  21.1 us (16%)
  other arithmetic  7.9 us (6%)
  local copies, waits for them, and re-layouts  5.96 us (4%)
    all_to_all x6, waiting for transfers between devices, swap(): return lax.all_to_all(values, axis, split_axis=0, concat_axis=0, tiled=True)  35 us
    all_to_all x6, starting transfers between devices, swap(): return lax.all_to_all(values, axis, split_axis=0, concat_axis=0, tiled=True)  27.6 us
    all_to_all x1, blocking collectives, swap(): return lax.all_to_all(values, axis, split_axis=0, concat_axis=0, tiled=True)  9.1 us
    all_gather x1, blocking collectives, local(): lax.all_gather(rows_part.reshape(rows_here, width_part), 'tp', axis=1, ti...  8.36 us
    all_to_all x1, waiting for transfers between devices, local(): lax.all_to_all(partial_value, 'tp', split_axis=1, concat_axis=0, tiled=True)  8.21 us
    all_gather x1, blocking collectives, local(): grads_full = lax.all_gather(cotangent, 'tp', axis=1, tiled=True)  5.97 us
    all_to_all x1, starting transfers between devices, local(): lax.all_to_all(partial_value, 'tp', split_axis=1, concat_axis=0, tiled=True)  3.48 us
    dot_general x1, matrix products, local(): lax.dot_general(weighted, grads_in, contract_rows, preferred_element_type...  3.3 us
  transfers between devices with their start and end apart: 7, of which 7 were waited for; matrix products, arithmetic and copies ran while one was open for 16% of the time, Pallas kernels for 0%

profile of v1, /device:TPU:0, one launch (start us, length us, event | category | flops | bytes accessed | tf_op | source)
XLA Modules:
  0.0 133.7 jit_solution(1982618690236708411)
XLA Ops:
  0.7 0.8 fusion.30
  1.5 0.1 convolution_select_fusion
  1.8 1.7 %convolution_convert_fusion.5 = bf16[320,256]{1,0:T(8,128)(2,1)} fusion(pred[320,128]{1,0:T(32,128)(4,1)S(1)} %bitcast_compare_fusion, bf16[128,256]{1,0:T(8,128)(2,1)} %param.9), kind=kOutput, calls=%fused_computation.21 | convolution fusion | flops 21053440 | bytes 270336 | tf_op jit(solution)/shard_map/dot_general | solution.py:48
  3.5 7.4 %all-to-all-start.2 = ((bf16[8,40,256]{2,1,0:T(8,128)(2,1)}), bf16[8,40,256]{2,1,0:T(8,128)(2,1)S(1)}, u32[]{:S(2)}, u32[]{:S(2)}) async-start(bf16[8,40,256]{2,1,0:T(8,128)(2,1)} %bitcast.7), calls=%async_computation.2 | async-start | bytes 327680 | tf_op jit(solution)/shard_map/all_to_all | solution.py:18
  10.9 6.0 %all_gather.6 = bf16[128,1024]{1,0:T(8,128)(2,1)S(1)} all-gather(bf16[128,256]{1,0:T(8,128)(2,1)} %param.10), channel_id=1, replica_groups=mesh['ep'=8,'tp'=4] {'tp'}, dimensions={1}, use_global_device_ids=true | all-gather | bytes 327680 | tf_op jit(solution)/shard_map/all_gather | solution.py:53
  16.9 1.2 convolution_convert_fusion.3
  18.1 0.4 all-to-all-done.2
  18.5 5.7 %all-to-all-start.1 = ((bf16[8,40,1024]{2,1,0:T(8,128)(2,1)}), bf16[8,40,1024]{2,1,0:T(8,128)(2,1)}, u32[]{:S(2)}, u32[]{:S(2)}) async-start(bf16[8,40,1024]{2,1,0:T(8,128)(2,1)} %bitcast.4), calls=%async_computation.1 | async-start | bytes 1310720 | tf_op jit(solution)/shard_map/all_to_all | solution.py:18
  24.2 0.3 convolution_bitcast_fusion
  24.5 8.4 %all_gather.7 = bf16[320,1024]{1,0:T(8,128)(2,1)} all-gather(bf16[320,256]{1,0:T(8,128)(2,1)S(1)} %bitcast.96), channel_id=1, replica_groups=mesh['ep'=8,'tp'=4] {'tp'}, dimensions={1}, use_global_device_ids=true | all-gather | bytes 819200 | tf_op jit(solution)/shard_map/all_gather | solution.py:55
  32.9 9.2 %all-to-all-done.1 = bf16[8,40,1024]{2,1,0:T(8,128)(2,1)} async-done(((bf16[8,40,1024]{2,1,0:T(8,128)(2,1)}), bf16[8,40,1024]{2,1,0:T(8,128)(2,1)}, u32[]{:S(2)}, u32[]{:S(2)}) %all-to-all-start.1) | async-done | bytes 655392 | tf_op jit(solution)/shard_map/all_to_all | solution.py:18
  42.1 0.9 broadcast_in_dim.99
  43.0 3.6 %all-to-all-start.5 = ((bf16[8,256,128]{2,1,0:T(8,128)(2,1)}), bf16[8,256,128]{2,1,0:T(8,128)(2,1)S(1)}, u32[]{:S(2)}, u32[]{:S(2)}) async-start(bf16[8,256,128]{2,1,0:T(8,128)(2,1)} %broadcast_in_dim.99), calls=%async_computation.5 | async-start | bytes 1048576 | tf_op jit(solution)/shard_map/all_to_all | solution.py:18
  46.7 1.9 %fusion.5 = f32[320,704]{1,0:T(8,128)S(1)} fusion(bf16[320,1024]{1,0:T(8,128)(2,1)} %all_gather.7, bf16[1,1024,704]{1,2,0:T(8,128)(2,1)S(1)} %copy-done), kind=kOutput, calls=%fused_computation.8 | convolution fusion | flops 461373440 | bytes 2998272 | tf_op jit(solution)/shard_map/dot_general | solution.py:69
  48.6 0.7 fusion.9
  49.4 0.2 copy-done.4
  49.6 0.9 copy-done.25
  50.4 2.8 %multiply_reduce_fusion = (f32[320]{0:T(512)S(1)}, f32[320,704]{1,0:T(8,128)}) fusion(f32[320,704]{1,0:T(8,128)S(1)} %fusion.9, f32[320,704]{1,0:T(8,128)S(1)} %fusion.5, bf16[320,1024]{1,0:T(8,128)(2,1)} %bitcast.5, bf16[1,704,1024]{2,1,0:T(8,128)(2,1)S(1)} %copy-done.25), kind=kOutput, calls=%fused_computation.31 | convolution fusion | flops 463400640 | bytes 4801792 | tf_op jit(solution)/shard_map/dot_general | solution.py:75
  53.4 7.9 %all-to-all-done.5 = bf16[8,256,128]{2,1,0:T(8,128)(2,1)S(1)} async-done(((bf16[8,256,128]{2,1,0:T(8,128)(2,1)}), bf16[8,256,128]{2,1,0:T(8,128)(2,1)S(1)}, u32[]{:S(2)}, u32[]{:S(2)}) %all-to-all-start.5) | async-done | bytes 524320 | tf_op jit(solution)/shard_map/all_to_all | solution.py:18
  61.5 0.8 broadcast_in_dim.104
  62.2 3.7 %all-to-all-start.6 = ((f32[32,1,1064]{2,1,0:T(1,128)}), f32[32,1,1064]{2,1,0:T(1,128)S(1)}, u32[]{:S(2)}, u32[]{:S(2)}) async-start(f32[32,1,1064]{2,1,0:T(1,128)} %broadcast_in_dim.104), calls=%async_computation.6 | async-start | bytes 294912 | tf_op jit(solution)/shard_map/all_to_all | solution.py:18
  66.0 8.4 %all-to-all-done.6 = f32[32,1,1064]{2,1,0:T(1,128)S(1)} async-done(((f32[32,1,1064]{2,1,0:T(1,128)}), f32[32,1,1064]{2,1,0:T(1,128)S(1)}, u32[]{:S(2)}, u32[]{:S(2)}) %all-to-all-start.6) | async-done | bytes 136224 | tf_op jit(solution)/shard_map/all_to_all | solution.py:18
  74.4 0.7 fusion.27
  75.1 9.1 %all_to_all.48 = bf16[8,1,40]{2,1,0:T(2,128)(2,1)S(1)} all-to-all(bf16[8,1,40]{2,1,0:T(2,128)(2,1)S(1)} %copy.32), channel_id=1, replica_groups=mesh['ep'=8,'tp'=4] {'ep'}, dimensions={0} | all-to-all | bytes 1280 | tf_op jit(solution)/shard_map/all_to_all | solution.py:18
  84.3 2.0 %multiply_convert_fusion.1 = (bf16[320,704]{1,0:T(8,128)(2,1)S(1)}, bf16[320,704]{1,0:T(8,128)(2,1)S(1)}) fusion(f32[320,704]{1,0:T(8,128)} %get-tuple-element.37, f32[320]{0:T(512)S(1)} %reshape.92, f32[320,704]{1,0:T(8,128)S(1)} %copy-done.5, f32[320,704]{1,0:T(8,128)} %copy-done.7), kind=kLoop, calls=%fused_computation.32 | loop fusion | flops 3153920 | bytes 3605760 | tf_op jit(solution)/shard_map/convert_element_type | solution.py:80
  86.4 0.7 fusion.3
  87.1 0.2 copy-done.1
  87.3 0.8 copy-done.3
  88.1 0.7 fusion.16
  88.8 0.9 copy.43
  89.7 3.5 %all-to-all-start.3 = ((bf16[320,4,256]{2,0,1:T(8,128)(2,1)}), bf16[320,4,256]{2,0,1:T(8,128)(2,1)S(1)}, u32[]{:S(2)}, u32[]{:S(2)}) async-start(bf16[320,4,256]{2,0,1:T(8,128)(2,1)} %bitcast.91), calls=%async_computation.3 | async-start | bytes 1310720 | tf_op jit(solution)/shard_map/all_to_all | solution.py:86
  93.2 1.1 convolution_convert_fusion.4
  94.3 0.2 copy.34
  94.5 0.6 slice_reduce_fusion
  95.2 8.2 %all-to-all-done.3 = bf16[320,4,256]{2,0,1:T(8,128)(2,1)S(1)} async-done(((bf16[320,4,256]{2,0,1:T(8,128)(2,1)}), bf16[320,4,256]{2,0,1:T(8,128)(2,1)S(1)}, u32[]{:S(2)}, u32[]{:S(2)}) %all-to-all-start.3) | async-done | bytes 655392 | tf_op jit(solution)/shard_map/all_to_all | solution.py:86
  103.4 3.5 %all-to-all-start.7 = ((bf16[8,256,128]{1,2,0:T(8,128)(2,1)}), bf16[8,256,128]{1,2,0:T(8,128)(2,1)S(1)}, u32[]{:S(2)}, u32[]{:S(2)}) async-start(bf16[8,256,128]{1,2,0:T(8,128)(2,1)} %bitcast.95), calls=%async_computation.7 | async-start | bytes 1048576 | tf_op jit(solution)/shard_map/all_to_all | solution.py:18
  106.9 1.4 %broadcast_multiply_fusion.1 = f32[1024]{0:T(1024)} fusion(f32[1024]{0:T(1024)} %slice_reduce_fusion), kind=kLoop, calls=%fused_computation.58 | loop fusion | flops 1024 | bytes 8192 | tf_op jit(solution)/shard_map/mul | solution.py:103
  108.3 1.3 select_reduce_fusion
  109.5 3.3 %fusion.1 = bf16[1,1024,704]{1,2,0:T(8,128)(2,1)} fusion(bf16[320,1024]{1,0:T(8,128)(2,1)} %all_gather.7, bf16[320,704]{1,0:T(8,128)(2,1)} %copy-done.1), kind=kOutput, calls=%fused_computation.4 | convolution fusion | flops 462094336 | bytes 2547712 | tf_op jit(solution)/shard_map/dot_general | solution.py:111
  112.9 2.1 %fusion = bf16[1,1024,704]{1,2,0:T(8,128)(2,1)} fusion(bf16[320,1024]{1,0:T(8,128)(2,1)S(1)} %copy-done.10, bf16[320,704]{1,0:T(8,128)(2,1)S(1)} %copy-done.14), kind=kOutput, calls=%fused_computation.3 | convolution fusion | flops 462094336 | bytes 2547712 | tf_op jit(solution)/shard_map/dot_general | solution.py:110
  114.9 3.3 %fusion.2 = bf16[1,704,1024]{2,1,0:T(8,128)(2,1)} fusion(bf16[320,1024]{1,0:T(8,128)(2,1)} %bitcast.5, f32[320]{0:T(512)S(1)} %copy-done.22, f32[320,704]{1,0:T(8,128)S(1)} %copy-done.8, f32[320,704]{1,0:T(8,128)S(1)} %copy-done.6), kind=kOutput, calls=%fused_computation.5 | convolution fusion | flops 463671296 | bytes 3900672 | tf_op jit(solution)/shard_map/dot_general | solution.py:112
  118.2 0.8 reduce_sum.95
  119.0 2.3 %all-to-all-done.7 = bf16[8,256,128]{1,2,0:T(8,128)(2,1)S(1)} async-done(((bf16[8,256,128]{1,2,0:T(8,128)(2,1)}), bf16[8,256,128]{1,2,0:T(8,128)(2,1)S(1)}, u32[]{:S(2)}, u32[]{:S(2)}) %all-to-all-start.7) | async-done | bytes 524320 | tf_op jit(solution)/shard_map/all_to_all | solution.py:18
  121.3 3.7 %all-to-all-start.4 = ((bf16[8,40,256]{2,1,0:T(8,128)(2,1)}), bf16[8,40,256]{2,1,0:T(8,128)(2,1)S(1)}, u32[]{:S(2)}, u32[]{:S(2)}) async-start(bf16[8,40,256]{2,1,0:T(8,128)(2,1)} %bitcast.97), calls=%async_computation.4 | async-start | bytes 327680 | tf_op jit(solution)/shard_map/all_to_all | solution.py:18
  125.0 0.8 copy.36
  125.8 6.8 %all-to-all-done.4 = bf16[8,40,256]{2,1,0:T(8,128)(2,1)S(1)} async-done(((bf16[8,40,256]{2,1,0:T(8,128)(2,1)}), bf16[8,40,256]{2,1,0:T(8,128)(2,1)S(1)}, u32[]{:S(2)}, u32[]{:S(2)}) %all-to-all-start.4) | async-done | bytes 163872 | tf_op jit(solution)/shard_map/all_to_all | solution.py:18
  132.5 0.3 convolution_bitcast_fusion.1
  132.9 0.9 fusion.19
  (69 shorter events, 0.8 us)
Async XLA Ops:
  0.6 46.0 %copy-start = (bf16[1,1024,704]{1,2,0:T(8,128)(2,1)S(1)}, bf16[1,1024,704]{1,2,0:T(8,128)(2,1)}, u32[]{:S(2)}) copy-start(bf16[1,1024,704]{1,2,0:T(8,128)(2,1)} %param.13) | copy-start | bytes 4325380
  0.7 73.7 %copy-start.23 = (f32[40]{0:T(128)}, f32[40]{0:T(128)S(1)}, u32[]{:S(2)}) copy-start(f32[40]{0:T(128)S(1)} %iota_convert_fusion) | copy-start | bytes 484
  1.6 72.8 %copy-start.16 = (f32[8,128]{1,0:T(8,128)}, f32[8,128]{1,0:T(8,128)S(1)}, u32[]{:S(2)}) copy-start(f32[8,128]{1,0:T(8,128)S(1)} %convolution_select_fusion) | copy-start | bytes 12292
  3.5 20.7 %copy-start.11 = (bf16[128,256]{1,0:T(8,128)(2,1)S(1)}, bf16[128,256]{1,0:T(8,128)(2,1)}, u32[]{:S(2)}) copy-start(bf16[128,256]{1,0:T(8,128)(2,1)} %param.9) | copy-start | bytes 196612
  3.5 15.0 %all-to-all-start.2 = ((bf16[8,40,256]{2,1,0:T(8,128)(2,1)}), bf16[8,40,256]{2,1,0:T(8,128)(2,1)S(1)}, u32[]{:S(2)}, u32[]{:S(2)}) async-start(bf16[8,40,256]{2,1,0:T(8,128)(2,1)} %bitcast.7), calls=%async_computation.2 | async-start | bytes 327680 | tf_op jit(solution)/shard_map/all_to_all | solution.py:18
  18.5 23.6 %copy-start.15 = (bf16[256,128]{1,0:T(8,128)(2,1)S(1)}, bf16[256,128]{1,0:T(8,128)(2,1)}, u32[]{:S(2)}) copy-start(bf16[256,128]{1,0:T(8,128)(2,1)} %param.16) | copy-start | bytes 196612
  18.5 23.6 %all-to-all-start.1 = ((bf16[8,40,1024]{2,1,0:T(8,128)(2,1)}), bf16[8,40,1024]{2,1,0:T(8,128)(2,1)}, u32[]{:S(2)}, u32[]{:S(2)}) async-start(bf16[8,40,1024]{2,1,0:T(8,128)(2,1)} %bitcast.4), calls=%async_computation.1 | async-start | bytes 1310720 | tf_op jit(solution)/shard_map/all_to_all | solution.py:18
  43.0 18.3 %all-to-all-start.5 = ((bf16[8,256,128]{2,1,0:T(8,128)(2,1)}), bf16[8,256,128]{2,1,0:T(8,128)(2,1)S(1)}, u32[]{:S(2)}, u32[]{:S(2)}) async-start(bf16[8,256,128]{2,1,0:T(8,128)(2,1)} %broadcast_in_dim.99), calls=%async_computation.5 | async-start | bytes 1048576 | tf_op jit(solution)/shard_map/all_to_all | solution.py:18
  46.6 2.0 %copy-start.2 = (bf16[1,1024,704]{1,2,0:T(8,128)(2,1)S(1)}, bf16[1,1024,704]{1,2,0:T(8,128)(2,1)}, u32[]{:S(2)}) copy-start(bf16[1,1024,704]{1,2,0:T(8,128)(2,1)} %param.14) | copy-start | bytes 4325380
  46.6 2.0 %copy-start.9 = (bf16[320,1024]{1,0:T(8,128)(2,1)S(1)}, bf16[320,1024]{1,0:T(8,128)(2,1)}, u32[]{:S(2)}) copy-start(bf16[320,1024]{1,0:T(8,128)(2,1)} %all_gather.7) | copy-start | bytes 1966084
  48.6 0.9 copy-start.4
  48.6 1.8 %copy-start.25 = (bf16[1,704,1024]{2,1,0:T(8,128)(2,1)S(1)}, bf16[1,704,1024]{2,1,0:T(8,128)(2,1)}, u32[]{:S(2)}) copy-start(bf16[1,704,1024]{2,1,0:T(8,128)(2,1)} %param.15) | copy-start | bytes 4325380
  49.4 3.9 %copy-start.7 = (f32[320,704]{1,0:T(8,128)}, f32[320,704]{1,0:T(8,128)S(1)}, u32[]{:S(2)}) copy-start(f32[320,704]{1,0:T(8,128)S(1)} %fusion.9) | copy-start | bytes 2703364
  53.3 12.6 %copy-start.26 = (bf16[128,2]{0,1:T(2,128)(2,1)S(1)}, bf16[128,2]{0,1:T(2,128)(2,1)}, u32[]{:S(2)}) copy-start(bf16[128,2]{0,1:T(2,128)(2,1)} %param.12) | copy-start | bytes 1540
  53.3 12.7 %copy-start.20 = (s32[128,2]{0,1:T(2,128)S(1)}, s32[128,2]{0,1:T(2,128)}, u32[]{:S(2)}) copy-start(s32[128,2]{0,1:T(2,128)} %param.11) | copy-start | bytes 3076
  61.4 22.9 %copy-start.5 = (f32[320,704]{1,0:T(8,128)S(1)}, f32[320,704]{1,0:T(8,128)}, u32[]{:S(2)}) copy-start(f32[320,704]{1,0:T(8,128)} %copy-done.4) | copy-start | bytes 2703364
  62.2 12.1 %all-to-all-start.6 = ((f32[32,1,1064]{2,1,0:T(1,128)}), f32[32,1,1064]{2,1,0:T(1,128)S(1)}, u32[]{:S(2)}, u32[]{:S(2)}) async-start(f32[32,1,1064]{2,1,0:T(1,128)} %broadcast_in_dim.104), calls=%async_computation.6 | async-start | bytes 294912 | tf_op jit(solution)/shard_map/all_to_all | solution.py:18
  84.3 2.0 %copy-start.21 = (f32[320]{0:T(512)}, f32[320]{0:T(512)S(1)}, u32[]{:S(2)}) copy-start(f32[320]{0:T(512)S(1)} %reshape.92) | copy-start | bytes 3844
  86.3 0.8 copy-start.13
  86.4 0.9 copy-start.1
  86.4 1.7 %copy-start.3 = (bf16[1,1024,704]{1,2,0:T(8,128)(2,1)S(1)}, bf16[1,1024,704]{1,2,0:T(8,128)(2,1)}, u32[]{:S(2)}) copy-start(bf16[1,1024,704]{1,2,0:T(8,128)(2,1)} %param.14) | copy-start | bytes 4325380
  88.8 4.4 %copy-start.12 = (bf16[128,256]{1,0:T(8,128)(2,1)S(1)}, bf16[128,256]{1,0:T(8,128)(2,1)}, u32[]{:S(2)}) copy-start(bf16[128,256]{1,0:T(8,128)(2,1)} %param.9) | copy-start | bytes 196612
  88.8 4.4 %copy-start.18 = (f32[1024]{0:T(1024)S(1)}, f32[1024]{0:T(1024)}, u32[]{:S(2)}) copy-start(f32[1024]{0:T(1024)} %param.17) | copy-start | bytes 12292
  89.7 13.7 %all-to-all-start.3 = ((bf16[320,4,256]{2,0,1:T(8,128)(2,1)}), bf16[320,4,256]{2,0,1:T(8,128)(2,1)S(1)}, u32[]{:S(2)}, u32[]{:S(2)}) async-start(bf16[320,4,256]{2,0,1:T(8,128)(2,1)} %bitcast.91), calls=%async_computation.3 | async-start | bytes 1310720 | tf_op jit(solution)/shard_map/all_to_all | solution.py:86
  103.4 17.9 %all-to-all-start.7 = ((bf16[8,256,128]{1,2,0:T(8,128)(2,1)}), bf16[8,256,128]{1,2,0:T(8,128)(2,1)S(1)}, u32[]{:S(2)}, u32[]{:S(2)}) async-start(bf16[8,256,128]{1,2,0:T(8,128)(2,1)} %bitcast.95), calls=%async_computation.7 | async-start | bytes 1048576 | tf_op jit(solution)/shard_map/all_to_all | solution.py:18
  106.9 6.0 %copy-start.10 = (bf16[320,1024]{1,0:T(8,128)(2,1)S(1)}, bf16[320,1024]{1,0:T(8,128)(2,1)}, u32[]{:S(2)}) copy-start(bf16[320,1024]{1,0:T(8,128)(2,1)} %all_gather.7) | copy-start | bytes 1966084
  106.9 6.0 %copy-start.14 = (bf16[320,704]{1,0:T(8,128)(2,1)S(1)}, bf16[320,704]{1,0:T(8,128)(2,1)}, u32[]{:S(2)}) copy-start(bf16[320,704]{1,0:T(8,128)(2,1)} %copy-done.13) | copy-start | bytes 1351684
  112.8 2.1 %copy-start.6 = (f32[320,704]{1,0:T(8,128)S(1)}, f32[320,704]{1,0:T(8,128)}, u32[]{:S(2)}) copy-start(f32[320,704]{1,0:T(8,128)} %copy-done.4) | copy-start | bytes 2703364
  112.8 2.1 %copy-start.8 = (f32[320,704]{1,0:T(8,128)S(1)}, f32[320,704]{1,0:T(8,128)}, u32[]{:S(2)}) copy-start(f32[320,704]{1,0:T(8,128)} %copy-done.7) | copy-start | bytes 2703364
  112.8 2.1 %copy-start.22 = (f32[320]{0:T(512)S(1)}, f32[320]{0:T(512)}, u32[]{:S(2)}) copy-start(f32[320]{0:T(512)} %copy-done.21) | copy-start | bytes 3844
  118.2 14.3 %copy-start.17 = (f32[8,128]{1,0:T(8,128)S(1)}, f32[8,128]{1,0:T(8,128)}, u32[]{:S(2)}) copy-start(f32[8,128]{1,0:T(8,128)} %copy-done.16) | copy-start | bytes 12292
  118.2 14.3 %copy-start.24 = (f32[40]{0:T(128)S(1)}, f32[40]{0:T(128)}, u32[]{:S(2)}) copy-start(f32[40]{0:T(128)} %copy-done.23) | copy-start | bytes 484
  118.2 14.6 %copy-start.19 = (f32[1024]{0:T(1024)S(1)}, f32[1024]{0:T(1024)}, u32[]{:S(2)}) copy-start(f32[1024]{0:T(1024)} %param.17) | copy-start | bytes 12292
  121.3 11.3 %all-to-all-start.4 = ((bf16[8,40,256]{2,1,0:T(8,128)(2,1)}), bf16[8,40,256]{2,1,0:T(8,128)(2,1)S(1)}, u32[]{:S(2)}, u32[]{:S(2)}) async-start(bf16[8,40,256]{2,1,0:T(8,128)(2,1)} %bitcast.97), calls=%async_computation.4 | async-start | bytes 327680 | tf_op jit(solution)/shard_map/all_to_all | solution.py:18

commit v2 on v1

--- a/solution.py
+++ b/solution.py
@@ -48,20 +48,25 @@
         taken = jnp.dot(dispatch, values, preferred_element_type=F32).astype(BF)
         return spread(taken.reshape(experts, capacity, values.shape[1]), group_size)
 
-    weights_in = swap(spread(slot_weight, group_size)[:, None, :], "ep").reshape(rows_here)
     rows_part = swap(pick(tokens), "ep")
     grads_full = lax.all_gather(cotangent, "tp", axis=1, tiled=True)
-    grads_in = swap(pick(grads_full), "ep").reshape(rows_here, width)
+    lanes = jnp.broadcast_to(spread(slot_weight, group_size)[:, :, None], (ep_count, capacity, 128))
+    arrived = swap(jnp.concatenate([pick(grads_full), lanes], axis=2), "ep")
+    arrived = arrived.reshape(rows_here, width + 128)
+    grads_in, weight_col = arrived[:, :width], arrived[:, width : width + 1].astype(F32)
     rows_in = lax.all_gather(rows_part.reshape(rows_here, width_part), "tp", axis=1, tiled=True)
 
-    dense_late, _ = lax.optimization_barrier((dense_weight, rows_part))
-    dense_cols = dense_late.shape[1]
-    gathered = swap(jnp.broadcast_to(dense_late[None], (ep_count,) + dense_late.shape), "ep")
-    scaled = (mix_gate[None, :] * grads_full.astype(F32)).astype(BF)
     contract_rows = (((0,), (0,)), ((), ()))
     contract_cols = (((1,), (1,)), ((), ()))
+    dense_cols = dense_weight.shape[1]
+    scaled = (mix_gate[None, :] * grads_full.astype(F32)).astype(BF)
     product = lax.dot_general(tokens, scaled, contract_rows, preferred_element_type=F32).astype(BF)
     product = product.reshape(width_part, ep_count, dense_cols).transpose(1, 0, 2)
+    copies = jnp.broadcast_to(dense_weight[None], (ep_count,) + dense_weight.shape)
+    outgoing, _ = lax.optimization_barrier((jnp.concatenate([copies, product], axis=1), arrived))
+    met = swap(outgoing, "ep")
+    gathered, shares = met[:, :width_part], met[:, width_part:]
+    dense_grad = jnp.sum(shares.astype(F32), axis=0) * (1.0 / ep_count)
 
     gate_matrix = w_gate[0]
     up_matrix = w_up[0]
@@ -74,7 +79,6 @@
     hidden_bf = hidden.astype(BF)
     projected = lax.dot_general(grads_in, down_matrix, contract_cols, preferred_element_type=F32)
     route_part = jnp.sum(hidden_bf.astype(F32) * projected, axis=1)
-    weight_col = weights_in.astype(F32)[:, None]
     hidden_grad = weight_col * projected
     d_gate = (hidden_grad * pre_up * sigmoid_gate * (1.0 + pre_gate * (1.0 - sigmoid_gate))).astype(BF)
     d_up = (hidden_grad * activated).astype(BF)
@@ -87,13 +91,10 @@
     column_sum = jnp.sum(mixed.reshape(tp_count, rows_here, -1).astype(F32), axis=0).astype(BF)
     returned = swap(column_sum.reshape(ep_count, capacity, width_part), "ep")
 
-    product_late, _ = lax.optimization_barrier((product, grads_in))
-    shares = swap(product_late, "ep")
-    dense_grad = jnp.sum(shares.astype(F32), axis=0) * (1.0 / ep_count)
-
     moment = lax.dot_general(tokens, grads_full, contract_rows, preferred_element_type=F32)
     moment = moment.reshape(width_part, ep_count, dense_cols)
     gain = jnp.sum(gathered.astype(F32) * moment.transpose(1, 0, 2), axis=1).reshape(1, width)
+    gain, route_part, _ = lax.optimization_barrier((gain, route_part, mixed))
     devices = ep_count * tp_count
     route_rows = jnp.broadcast_to(
         route_part.reshape(ep_count, 1, capacity), (ep_count, tp_count, capacity)

time: 135 us -> 123 us (0.911)
  blocking collectives: 23.4 us -> 13.9 us
  starting transfers between devices: 31.1 us -> 27.1 us
  waiting for transfers between devices: 43.2 us -> 45.5 us
  local copies, waits for them, and re-layouts: 5.96 us -> 3.72 us
    all_to_all x1 -> x0, blocking collectives: 9.1 us -> none  [swap(): return lax.all_to_all(values, axis, split_axis=0, concat_axis=0, tiled=True)]
    all_to_all x6 -> x5, starting transfers between devices: 27.6 us -> 23.5 us  [swap(): return lax.all_to_all(values, axis, split_axis=0, concat_axis=0, tiled=True)]
    convert_element_type x2 -> x0, other arithmetic: 2.01 us -> none  [the longest x1 2 us: local(): d_up = (hidden_grad * activated).astype(BF)]
    concatenate x0 -> x2, other arithmetic: none -> 2 us  [the longest x1 1.08 us: local(): jnp.concatenate([copies, product], axis=1)]
    all_to_all x1, waiting for transfers between devices: 8.21 us -> 10.1 us  [local(): lax.all_to_all(partial_value, 'tp', split_axis=1, concat_axis=0, tiled=True)]
    reduce_sum x1, other arithmetic: 0.07 us -> 1.48 us  [local(): dense_grad = jnp.sum(shares.astype(F32), axis=0) * (1.0 / ep_count)]
    reshape x0 -> x1, matrix products: none -> 1.38 us  [local(): moment = moment.reshape(width_part, ep_count, dense_cols)]
    unnamed x56 -> x33, local copies, waits for them, and re-layouts: 2.98 us -> 1.85 us
  transfers between devices with their start and end apart: 7 -> 6, of which waited for: 7 -> 5; matrix products, arithmetic and copies ran while one was open for 16% -> 16% of each run, Pallas kernels for 0% -> 0%
where the time goes in v2:
time: 123 us; the launch traced here: 122 us
  waiting for transfers between devices  45.5 us (37%)
  starting transfers between devices  27.1 us (22%)
  matrix products  21.6 us (18%)
  blocking collectives  13.9 us (11%)
  other arithmetic  9.05 us (7%)
  local copies, waits for them, and re-layouts  3.72 us (3%)
    all_to_all x5, waiting for transfers between devices, swap(): return lax.all_to_all(values, axis, split_axis=0, concat_axis=0, tiled=True)  35.5 us
    all_to_all x5, starting transfers between devices, swap(): return lax.all_to_all(values, axis, split_axis=0, concat_axis=0, tiled=True)  23.5 us
    all_to_all x1, waiting for transfers between devices, local(): lax.all_to_all(partial_value, 'tp', split_axis=1, concat_axis=0, tiled=True)  10.1 us
    all_gather x1, blocking collectives, local(): lax.all_gather(rows_part.reshape(rows_here, width_part), 'tp', axis=1, ti...  7.9 us
    all_gather x1, blocking collectives, local(): grads_full = lax.all_gather(cotangent, 'tp', axis=1, tiled=True)  5.97 us
    all_to_all x1, starting transfers between devices, local(): lax.all_to_all(partial_value, 'tp', split_axis=1, concat_axis=0, tiled=True)  3.61 us
    dot_general x1, matrix products, local(): lax.dot_general(weighted, grads_in, contract_rows, preferred_element_type...  3.32 us
    dot_general x1, matrix products, local(): lax.dot_general(grads_in, down_matrix, contract_cols, preferred_element_t...  3.28 us
  transfers between devices with their start and end apart: 6, of which 5 were waited for; matrix products, arithmetic and copies ran while one was open for 16% of the time, Pallas kernels for 0%

profile of v2, /device:TPU:0, one launch (start us, length us, event | category | flops | bytes accessed | tf_op | source)
XLA Modules:
  0.0 121.8 jit_solution(18386872155913374480)
XLA Ops:
  0.7 0.8 fusion.46
  1.5 0.1 convolution_select_fusion
  1.7 0.1 bitcast_compare_fusion
  1.8 1.7 %convolution_convert_fusion.5 = bf16[320,256]{1,0:T(8,128)(2,1)} fusion(pred[320,128]{1,0:T(32,128)(4,1)S(1)} %bitcast_compare_fusion, bf16[128,256]{1,0:T(8,128)(2,1)} %param.9), kind=kOutput, calls=%fused_computation.20 | convolution fusion | flops 21053440 | bytes 270336 | tf_op jit(solution)/shard_map/dot_general | solution.py:48
  3.5 7.3 %all-to-all-start.1 = ((bf16[8,40,256]{2,1,0:T(8,128)(2,1)}), bf16[8,40,256]{2,1,0:T(8,128)(2,1)S(1)}, u32[]{:S(2)}, u32[]{:S(2)}) async-start(bf16[8,40,256]{2,1,0:T(8,128)(2,1)} %bitcast.6), calls=%async_computation.1 | async-start | bytes 327680 | tf_op jit(solution)/shard_map/all_to_all | solution.py:18
  10.8 0.7 convert_element_type.82
  11.4 0.7 select_reduce_fusion.1
  12.1 6.0 %all_gather.6 = bf16[128,1024]{1,0:T(8,128)(2,1)S(1)} all-gather(bf16[128,256]{1,0:T(8,128)(2,1)} %param.10), channel_id=1, replica_groups=mesh['ep'=8,'tp'=4] {'tp'}, dimensions={1}, use_global_device_ids=true | all-gather | bytes 327680 | tf_op jit(solution)/shard_map/all_gather | solution.py:52
  18.1 0.3 convolution_convert_fusion.3
  18.4 0.2 fusion.27
  18.6 0.9 pad_maximum_fusion.1
  19.5 6.1 %all-to-all-start = ((bf16[8,40,1152]{2,1,0:T(8,128)(2,1)}), bf16[8,40,1152]{2,1,0:T(8,128)(2,1)}, u32[]{:S(2)}, u32[]{:S(2)}) async-start(bf16[8,40,1152]{2,1,0:T(8,128)(2,1)} %pad_maximum_fusion.1), calls=%async_computation | async-start | bytes 1474560 | tf_op jit(solution)/shard_map/all_to_all | solution.py:18
  25.7 7.9 %all_gather.7 = bf16[320,1024]{1,0:T(8,128)(2,1)S(1)} all-gather(bf16[320,256]{1,0:T(8,128)(2,1)S(1)} %bitcast.83), channel_id=1, replica_groups=mesh['ep'=8,'tp'=4] {'tp'}, dimensions={1}, use_global_device_ids=true | all-gather | bytes 819200 | tf_op jit(solution)/shard_map/all_gather | solution.py:57
  33.6 1.7 %fusion.9 = f32[320,704]{1,0:T(8,128)} fusion(bf16[320,1024]{1,0:T(8,128)(2,1)S(1)} %all_gather.7, bf16[1,1024,704]{1,2,0:T(8,128)(2,1)S(1)} %copy-done.1), kind=kOutput, calls=%fused_computation.12 | convolution fusion | flops 461373440 | bytes 2998272 | tf_op jit(solution)/shard_map/dot_general | solution.py:75
  35.3 1.7 %fusion.5 = f32[320,704]{1,0:T(8,128)} fusion(bf16[320,1024]{1,0:T(8,128)(2,1)S(1)} %all_gather.7, bf16[1,1024,704]{1,2,0:T(8,128)(2,1)S(1)} %copy-done), kind=kOutput, calls=%fused_computation.8 | convolution fusion | flops 461373440 | bytes 2998272 | tf_op jit(solution)/shard_map/dot_general | solution.py:74
  37.0 8.4 %all-to-all-done = bf16[8,40,1152]{2,1,0:T(8,128)(2,1)} async-done(((bf16[8,40,1152]{2,1,0:T(8,128)(2,1)}), bf16[8,40,1152]{2,1,0:T(8,128)(2,1)}, u32[]{:S(2)}, u32[]{:S(2)}) %all-to-all-start) | async-done | bytes 737312 | tf_op jit(solution)/shard_map/all_to_all | solution.py:18
  45.4 1.0 convert_reduce_fusion.1
  46.4 3.3 %multiply_reduce_fusion.1 = (f32[320]{0:T(512)S(1)}, bf16[320,704]{1,0:T(8,128)(2,1)S(1)}, bf16[320,704]{1,0:T(8,128)(2,1)S(1)}) fusion(f32[320,704]{1,0:T(8,128)} %fusion.9, f32[320,704]{1,0:T(8,128)} %fusion.5, f32[320]{0:T(512)S(1)} %convert_reduce_fusion.1, bf16[1,704,1024]{2,1,0:T(8,128)(2,1)} %param.15, bf16[320,1152]{1,0:T(8,128)(2,1)} %bitcast.4), kind=kOutput, calls=%fused_computation.29 | convolution fusion | flops 465653440 | bytes 4966912 | tf_op jit(solution)/shard_map/dot_general | solution.py:80
  49.7 0.7 fusion.3
  50.4 0.1 copy-done.14
  50.5 0.2 copy-done.7
  50.6 0.7 fusion.16
  51.3 0.9 copy.45
  52.2 3.6 %all-to-all-start.2 = ((bf16[320,4,256]{2,0,1:T(8,128)(2,1)}), bf16[320,4,256]{2,0,1:T(8,128)(2,1)S(1)}, u32[]{:S(2)}, u32[]{:S(2)}) async-start(bf16[320,4,256]{2,0,1:T(8,128)(2,1)} %bitcast.76), calls=%async_computation.2 | async-start | bytes 1310720 | tf_op jit(solution)/shard_map/all_to_all | solution.py:90
  55.9 0.1 copy.37
  56.0 10.1 %all-to-all-done.2 = bf16[320,4,256]{2,0,1:T(8,128)(2,1)S(1)} async-done(((bf16[320,4,256]{2,0,1:T(8,128)(2,1)}), bf16[320,4,256]{2,0,1:T(8,128)(2,1)S(1)}, u32[]{:S(2)}, u32[]{:S(2)}) %all-to-all-start.2) | async-done | bytes 655392 | tf_op jit(solution)/shard_map/all_to_all | solution.py:90
  66.0 0.8 reduce_sum.95
  66.8 3.6 %all-to-all-start.3 = ((bf16[8,40,256]{2,1,0:T(8,128)(2,1)}), bf16[8,40,256]{2,1,0:T(8,128)(2,1)S(1)}, u32[]{:S(2)}, u32[]{:S(2)}) async-start(bf16[8,40,256]{2,1,0:T(8,128)(2,1)} %bitcast.10), calls=%async_computation.3 | async-start | bytes 327680 | tf_op jit(solution)/shard_map/all_to_all | solution.py:18
  70.5 0.3 convolution_convert_fusion.4
  70.9 1.1 pad_maximum_fusion
  71.9 6.1 %all-to-all-done.3 = bf16[8,40,256]{2,1,0:T(8,128)(2,1)S(1)} async-done(((bf16[8,40,256]{2,1,0:T(8,128)(2,1)}), bf16[8,40,256]{2,1,0:T(8,128)(2,1)S(1)}, u32[]{:S(2)}, u32[]{:S(2)}) %all-to-all-start.3) | async-done | bytes 163872 | tf_op jit(solution)/shard_map/all_to_all | solution.py:18
  78.0 0.7 copy-done.4
  78.7 3.6 %all-to-all-start.4 = ((bf16[8,512,128]{1,2,0:T(8,128)(2,1)}), bf16[8,512,128]{1,2,0:T(8,128)(2,1)S(1)}, u32[]{:S(2)}, u32[]{:S(2)}) async-start(bf16[8,512,128]{1,2,0:T(8,128)(2,1)} %pad_maximum_fusion), calls=%async_computation.4 | async-start | bytes 2097152 | tf_op jit(solution)/shard_map/all_to_all | solution.py:18
  82.2 1.4 %fusion.55 = f32[256,1024]{0,1:T(8,128)} fusion(bf16[128,256]{1,0:T(8,128)(2,1)S(1)} %copy-done.6, bf16[128,1024]{1,0:T(8,128)(2,1)S(1)} %all_gather.6), kind=kOutput, calls=%fused_computation.84 | convolution fusion | flops 67108864 | bytes 1376256 | tf_op jit(solution)/shard_map/reshape | solution.py:95
  83.6 3.2 %fusion = bf16[1,1024,704]{1,2,0:T(8,128)(2,1)} fusion(bf16[320,1024]{1,0:T(8,128)(2,1)S(1)} %copy-done.3, bf16[320,704]{1,0:T(8,128)(2,1)} %copy-done.14), kind=kOutput, calls=%fused_computation.3 | convolution fusion | flops 462094336 | bytes 2547712 | tf_op jit(solution)/shard_map/dot_general | solution.py:111
  86.8 2.1 %fusion.1 = bf16[1,1024,704]{1,2,0:T(8,128)(2,1)} fusion(bf16[320,1024]{1,0:T(8,128)(2,1)S(1)} %copy-done.3, bf16[320,704]{1,0:T(8,128)(2,1)S(1)} %copy-done.8), kind=kOutput, calls=%fused_computation.4 | convolution fusion | flops 462094336 | bytes 2547712 | tf_op jit(solution)/shard_map/dot_general | solution.py:112
  88.9 3.3 %fusion.2 = bf16[1,704,1024]{2,1,0:T(8,128)(2,1)} fusion(bf16[320,1152]{1,0:T(8,128)(2,1)} %bitcast.4, f32[320]{0:T(512)S(1)} %convert_reduce_fusion.1, f32[320,704]{1,0:T(8,128)S(1)} %copy-done.12, f32[320,704]{1,0:T(8,128)S(1)} %copy-done.13), kind=kOutput, calls=%fused_computation.5 | convolution fusion | flops 463671296 | bytes 3900672 | tf_op jit(solution)/shard_map/dot_general | solution.py:113
  92.2 0.3 convolution_bitcast_fusion
  92.5 14.3 %all-to-all-done.4 = bf16[8,512,128]{1,2,0:T(8,128)(2,1)S(1)} async-done(((bf16[8,512,128]{1,2,0:T(8,128)(2,1)}), bf16[8,512,128]{1,2,0:T(8,128)(2,1)S(1)}, u32[]{:S(2)}, u32[]{:S(2)}) %all-to-all-start.4) | async-done | bytes 1048608 | tf_op jit(solution)/shard_map/all_to_all | solution.py:18
  106.8 1.5 %convert_reduce_fusion = (f32[256,128]{0,1:T(8,128)S(1)}, f32[8,128]{1,0:T(8,128)S(1)}) fusion(bf16[8,512,128]{1,2,0:T(8,128)(2,1)S(1)} %all-to-all-done.4, f32[8,256,128]{1,2,0:T(8,128)} %bitcast.78), kind=kLoop, calls=%fused_computation.26 | loop fusion | flops 1276928 | bytes 2232320 | tf_op jit(solution)/shard_map/reduce_sum | solution.py:69
  108.4 0.8 broadcast_in_dim.108
  109.1 2.9 %all-to-all-start.5 = ((f32[32,1,1064]{2,1,0:T(1,128)}), f32[32,1,1064]{2,1,0:T(1,128)S(1)}, u32[]{:S(2)}, u32[]{:S(2)}) async-start(f32[32,1,1064]{2,1,0:T(1,128)} %broadcast_in_dim.108), calls=%async_computation.5 | async-start | bytes 294912 | tf_op jit(solution)/shard_map/all_to_all | solution.py:18
  112.1 0.8 copy.39
  112.9 0.9 fusion.19
  113.7 6.7 %all-to-all-done.5 = f32[32,1,1064]{2,1,0:T(1,128)S(1)} async-done(((f32[32,1,1064]{2,1,0:T(1,128)}), f32[32,1,1064]{2,1,0:T(1,128)S(1)}, u32[]{:S(2)}, u32[]{:S(2)}) %all-to-all-start.5) | async-done | bytes 136224 | tf_op jit(solution)/shard_map/all_to_all | solution.py:18
  120.5 0.1 fusion.29
  120.7 0.6 select_reduce_fusion
  121.2 0.6 broadcast_multiply_fusion.1
  (42 shorter events, 0.4 us)
Async XLA Ops:
  0.6 34.6 %copy-start = (bf16[1,1024,704]{1,2,0:T(8,128)(2,1)S(1)}, bf16[1,1024,704]{1,2,0:T(8,128)(2,1)}, u32[]{:S(2)}) copy-start(bf16[1,1024,704]{1,2,0:T(8,128)(2,1)} %param.13) | copy-start | bytes 4325380
  3.5 16.0 %all-to-all-start.1 = ((bf16[8,40,256]{2,1,0:T(8,128)(2,1)}), bf16[8,40,256]{2,1,0:T(8,128)(2,1)S(1)}, u32[]{:S(2)}, u32[]{:S(2)}) async-start(bf16[8,40,256]{2,1,0:T(8,128)(2,1)} %bitcast.6), calls=%async_computation.1 | async-start | bytes 327680 | tf_op jit(solution)/shard_map/all_to_all | solution.py:18
  19.5 14.0 %copy-start.1 = (bf16[1,1024,704]{1,2,0:T(8,128)(2,1)S(1)}, bf16[1,1024,704]{1,2,0:T(8,128)(2,1)}, u32[]{:S(2)}) copy-start(bf16[1,1024,704]{1,2,0:T(8,128)(2,1)} %param.14) | copy-start | bytes 4325380
  19.5 25.8 %all-to-all-start = ((bf16[8,40,1152]{2,1,0:T(8,128)(2,1)}), bf16[8,40,1152]{2,1,0:T(8,128)(2,1)}, u32[]{:S(2)}, u32[]{:S(2)}) async-start(bf16[8,40,1152]{2,1,0:T(8,128)(2,1)} %pad_maximum_fusion.1), calls=%async_computation | async-start | bytes 1474560 | tf_op jit(solution)/shard_map/all_to_all | solution.py:18
  33.6 1.7 %copy-start.2 = (bf16[320,1024]{1,0:T(8,128)(2,1)}, bf16[320,1024]{1,0:T(8,128)(2,1)S(1)}, u32[]{:S(2)}) copy-start(bf16[320,1024]{1,0:T(8,128)(2,1)S(1)} %all_gather.7) | copy-start | bytes 1966084
  49.7 0.8 copy-start.14
  49.7 1.0 copy-start.7
  51.3 4.5 %copy-start.9 = (bf16[256,128]{1,0:T(8,128)(2,1)S(1)}, bf16[256,128]{1,0:T(8,128)(2,1)}, u32[]{:S(2)}) copy-start(bf16[256,128]{1,0:T(8,128)(2,1)} %param.16) | copy-start | bytes 196612
  52.2 18.2 %copy-start.6 = (bf16[128,256]{1,0:T(8,128)(2,1)S(1)}, bf16[128,256]{1,0:T(8,128)(2,1)}, u32[]{:S(2)}) copy-start(bf16[128,256]{1,0:T(8,128)(2,1)} %param.9) | copy-start | bytes 196612
  52.2 18.2 %copy-start.10 = (f32[1024]{0:T(1024)S(1)}, f32[1024]{0:T(1024)}, u32[]{:S(2)}) copy-start(f32[1024]{0:T(1024)} %param.17) | copy-start | bytes 12292
  52.2 13.8 %all-to-all-start.2 = ((bf16[320,4,256]{2,0,1:T(8,128)(2,1)}), bf16[320,4,256]{2,0,1:T(8,128)(2,1)S(1)}, u32[]{:S(2)}, u32[]{:S(2)}) async-start(bf16[320,4,256]{2,0,1:T(8,128)(2,1)} %bitcast.76), calls=%async_computation.2 | async-start | bytes 1310720 | tf_op jit(solution)/shard_map/all_to_all | solution.py:90
  66.8 11.2 %all-to-all-start.3 = ((bf16[8,40,256]{2,1,0:T(8,128)(2,1)}), bf16[8,40,256]{2,1,0:T(8,128)(2,1)S(1)}, u32[]{:S(2)}, u32[]{:S(2)}) async-start(bf16[8,40,256]{2,1,0:T(8,128)(2,1)} %bitcast.10), calls=%async_computation.3 | async-start | bytes 327680 | tf_op jit(solution)/shard_map/all_to_all | solution.py:18
  71.9 11.7 %copy-start.3 = (bf16[320,1024]{1,0:T(8,128)(2,1)S(1)}, bf16[320,1024]{1,0:T(8,128)(2,1)}, u32[]{:S(2)}) copy-start(bf16[320,1024]{1,0:T(8,128)(2,1)} %copy-done.2) | copy-start | bytes 1966084
  78.0 0.7 copy-start.4
  78.7 28.1 %all-to-all-start.4 = ((bf16[8,512,128]{1,2,0:T(8,128)(2,1)}), bf16[8,512,128]{1,2,0:T(8,128)(2,1)S(1)}, u32[]{:S(2)}, u32[]{:S(2)}) async-start(bf16[8,512,128]{1,2,0:T(8,128)(2,1)} %pad_maximum_fusion), calls=%async_computation.4 | async-start | bytes 2097152 | tf_op jit(solution)/shard_map/all_to_all | solution.py:18
  83.6 3.2 %copy-start.8 = (bf16[320,704]{1,0:T(8,128)(2,1)S(1)}, bf16[320,704]{1,0:T(8,128)(2,1)}, u32[]{:S(2)}) copy-start(bf16[320,704]{1,0:T(8,128)(2,1)} %copy-done.7) | copy-start | bytes 1351684
  86.8 2.1 %copy-start.12 = (f32[320,704]{1,0:T(8,128)S(1)}, f32[320,704]{1,0:T(8,128)}, u32[]{:S(2)}) copy-start(f32[320,704]{1,0:T(8,128)} %fusion.9) | copy-start | bytes 2703364
  86.8 2.1 %copy-start.13 = (f32[320,704]{1,0:T(8,128)S(1)}, f32[320,704]{1,0:T(8,128)}, u32[]{:S(2)}) copy-start(f32[320,704]{1,0:T(8,128)} %fusion.5) | copy-start | bytes 2703364
  88.9 3.3 %copy-start.5 = (bf16[8,40,256]{2,1,0:T(8,128)(2,1)S(1)}, bf16[8,40,256]{2,1,0:T(8,128)(2,1)}, u32[]{:S(2)}) copy-start(bf16[8,40,256]{2,1,0:T(8,128)(2,1)} %copy-done.4) | copy-start | bytes 491524
  109.1 11.3 %all-to-all-start.5 = ((f32[32,1,1064]{2,1,0:T(1,128)}), f32[32,1,1064]{2,1,0:T(1,128)S(1)}, u32[]{:S(2)}, u32[]{:S(2)}) async-start(f32[32,1,1064]{2,1,0:T(1,128)} %broadcast_in_dim.108), calls=%async_computation.5 | async-start | bytes 294912 | tf_op jit(solution)/shard_map/all_to_all | solution.py:18
  112.0 8.6 %copy-start.11 = (s32[128,2]{0,1:T(2,128)S(1)}, s32[128,2]{0,1:T(2,128)}, u32[]{:S(2)}) copy-start(s32[128,2]{0,1:T(2,128)} %param.11) | copy-start | bytes 3076
